TPU v7x, 32 devices: a whole 2x2x4 slice. The times are simulated.
32 devices in a mesh: ep: 8 (over z, x), tp: 4 (over y, core).
Axes of the slice: x: 2, y: 2, z: 4, core: 2. Of those that a mesh axis runs over, the one named last changes fastest.
Arguments:
- tokens_first: bfloat16 [4096, 2048], P('ep'), may hold values from -6 to 6
- attn_gain: float32 [2048], replicated, may hold values from 0.1 to 1.9
- w_query: bfloat16 [2048, 1024], P(None, 'tp'), may hold values from -6 to 6
- key_matrix: bfloat16 [2048, 512], P(None, 'tp'), may hold values from -6 to 6
- value_matrix: bfloat16 [2048, 512], P(None, 'tp'), may hold values from -0.125 to 0.125
- head_sink_logit: float32 [16], P('tp'), may hold values from 1 to 5
- w_output: bfloat16 [1024, 2048], P('tp'), may hold values from -0.75 to 0.75
- tokens_second: bfloat16 [1024, 2048], P('ep'), may hold values from -6 to 6
- ffn_gain: float32 [2048], replicated, may hold values from 0.1 to 1.9
- routes: int32 [1024, 4], P('ep'), may hold values from 0 to 15, all different within a row; in each aligned block of 128 rows (0 to 127, 128 to 255, ...) at most 64 rows name the same one
- route_weight: float32 [1024, 4], P('ep'), may hold values from 0.2 to 1.5
- w_gate_exp: bfloat16 [16, 2048, 2048], P('ep', None, 'tp'), may hold values from -0.125 to 0.125
- w_up_exp: bfloat16 [16, 2048, 2048], P('ep', None, 'tp'), may hold values from -0.125 to 0.125
- w_down_exp: bfloat16 [16, 2048, 2048], P('ep', 'tp'), may hold values from -0.125 to 0.125
- w_gate_shared: bfloat16 [2048, 1024], P(None, 'tp'), may hold values from -0.125 to 0.125
- w_up_shared: bfloat16 [2048, 1024], P(None, 'tp'), may hold values from -0.125 to 0.125
- w_down_shared: bfloat16 [1024, 2048], P('tp'), may hold values from -0.1875 to 0.1875
Outputs:
- mixer_out: bfloat16 [4096, 2048], P(('ep', 'tp'))
- moe_out: bfloat16 [1024, 2048], P('ep', 'tp')
Inputs may be any that keep to these rules, and one draw needn't show every extreme that they name: `routes`: each row names 4 different experts; among the rows of one index of ep no expert is named more than 64 times, a bound that some block reaches.
All inputs are finite; a program needn't handle non-finite values.
Results may differ from a plain program's by a relative error of at most 0.017.
Values may be sent and summed in bfloat16 or wider, within the bound.
No kernel may reach another device: no remote copies, remote signals or barrier semaphores. Data moves between devices by JAX's collectives and lax.ppermute only.
A program may use at most 64 MiB of HBM per device.

v0:
```python
import jax
import jax.numpy as jnp
from jax import lax
from jax.sharding import PartitionSpec as P

MODEL_WIDTH = 2048
HEAD_SIZE = 64
BAND_LENGTH = 128
rope_base = 10000.0
norm_eps = 1e-06


def from_behind(value, axis, by):
    devices = lax.axis_size(axis)
    pairs = [(i, i + by) for i in range(devices) if 0 <= i + by < devices]
    return lax.ppermute(value, axis, pairs)


def rms_scale(inputs, gain):
    wide = inputs.astype(jnp.float32)
    scaled = wide * lax.rsqrt(jnp.mean(wide * wide, axis=-1, keepdims=True) + norm_eps)
    return (scaled * gain).astype(jnp.bfloat16)


def apply_rotary(heads, token_positions):
    freqs = rope_base ** (-jnp.arange(0, HEAD_SIZE, 2, dtype=jnp.float32) / HEAD_SIZE)
    angles = token_positions[:, None] * freqs[None, :]
    cosine = jnp.cos(angles)[:, None, :]
    sine = jnp.sin(angles)[:, None, :]
    first_half, second_half = jnp.split(heads, 2, axis=-1)
    return jnp.concatenate(
        [first_half * cosine - second_half * sine, second_half * cosine + first_half * sine],
        axis=-1,
    )


def local(
    tokens_first,
    attn_gain,
    w_query,
    key_matrix,
    value_matrix,
    head_sink_logit,
    w_output,
    tokens_second,
    ffn_gain,
    routes,
    route_weight,
    w_gate_exp,
    w_up_exp,
    w_down_exp,
    w_gate_shared,
    w_up_shared,
    w_down_shared,
):
    rows_first = tokens_first.shape[0]
    norm_input = rms_scale(tokens_first, attn_gain)
    offset = lax.axis_index("ep") * rows_first
    token_positions = (offset + jnp.arange(rows_first, dtype=jnp.int32)).astype(jnp.float32)
    head_count = w_query.shape[1] // HEAD_SIZE
    key_heads = key_matrix.shape[1] // HEAD_SIZE
    head_group = head_count // key_heads
    query_rows = apply_rotary(
        jnp.dot(norm_input, w_query, preferred_element_type=jnp.float32).reshape(
            rows_first, head_count, HEAD_SIZE
        ),
        token_positions,
    ).astype(jnp.bfloat16)
    keys_local = apply_rotary(
        jnp.dot(norm_input, key_matrix, preferred_element_type=jnp.float32).reshape(
            rows_first, key_heads, HEAD_SIZE
        ),
        token_positions,
    ).astype(jnp.bfloat16)
    values_local = (
        jnp.dot(norm_input, value_matrix, preferred_element_type=jnp.float32)
        .astype(jnp.bfloat16)
        .reshape(rows_first, key_heads, HEAD_SIZE)
    )
    keys_before, values_before = from_behind(
        (keys_local[rows_first - BAND_LENGTH :], values_local[rows_first - BAND_LENGTH :]), "ep", 1
    )
    keys_all = jnp.concatenate([keys_before, keys_local], axis=0)
    values_all = jnp.concatenate([values_before, values_local], axis=0)
    layer_block = min(512, rows_first)
    sink_scores = head_sink_logit.reshape(key_heads, head_group)[:, :, None, None]

    def attend(index):
        leading_row = index * layer_block
        block_queries = query_rows.reshape(layer_block, key_heads, head_group, HEAD_SIZE)
        scores = jnp.einsum(
            "qhgd,khd->hgqk", block_queries, keys_all, preferred_element_type=jnp.float32
        ) * HEAD_SIZE ** (-0.5)
        query_pos = offset + leading_row + jnp.arange(layer_block, dtype=jnp.int32)
        key_pos = (
            offset
            + leading_row
            - BAND_LENGTH
            + jnp.arange(layer_block + BAND_LENGTH, dtype=jnp.int32)
        )
        offsets = query_pos[:, None] - key_pos[None, :]
        visible = (offsets >= 0) & (offsets < BAND_LENGTH) & (key_pos[None, :] >= 0)
        scores = jnp.where(visible[None, None], scores, -jnp.inf)
        peak = jnp.maximum(jnp.max(scores, axis=-1, keepdims=True), sink_scores)
        expo = jnp.exp(scores - peak)
        total = jnp.sum(expo, axis=-1, keepdims=True) + jnp.exp(sink_scores - peak)
        weights = (expo / total).astype(jnp.bfloat16)
        mixed = jnp.einsum(
            "hgqk,khd->qhgd", weights, values_all, preferred_element_type=jnp.float32
        )
        return mixed.astype(jnp.bfloat16).reshape(layer_block, head_count * HEAD_SIZE)

    attended = lax.map(attend, jnp.arange(rows_first // layer_block, dtype=jnp.int32)).reshape(
        rows_first, head_count * HEAD_SIZE
    )
    mixer_out = lax.psum_scatter(
        jnp.dot(attended, w_output, preferred_element_type=jnp.float32).astype(jnp.bfloat16),
        "tp",
        scatter_dimension=0,
        tiled=True,
    )
    rows_second = tokens_second.shape[0]
    topk = routes.shape[1]
    exp_dev = w_gate_exp.shape[0]
    n_expdev = lax.axis_size("ep")
    experts = exp_dev * n_expdev
    capacity = max(2, 2 * rows_second * topk // experts)
    slot_count = experts * capacity
    normed_second = rms_scale(tokens_second, ffn_gain)
    flat = routes.reshape(-1)
    onehot = (flat[:, None] == jnp.arange(experts, dtype=jnp.int32)[None, :]).astype(jnp.int32)
    ranks = jnp.sum((jnp.cumsum(onehot, axis=0) - onehot) * onehot, axis=1)
    slots = flat * capacity + ranks
    match = (jnp.arange(slot_count, dtype=jnp.int32)[:, None] == slots[None, :]).reshape(
        slot_count, rows_second, topk
    )
    dispatch = jnp.sum(match.astype(jnp.float32), axis=2).astype(jnp.bfloat16)
    combine = jnp.sum(match.astype(jnp.float32) * route_weight[None, :, :], axis=2)
    width = normed_second.shape[1] // lax.axis_size("tp")
    feature_slice = lax.dynamic_slice_in_dim(normed_second, lax.axis_index("tp") * width, width, 1)
    outgoing = jnp.dot(dispatch, feature_slice, preferred_element_type=jnp.float32).astype(
        jnp.bfloat16
    )
    arrived = lax.all_to_all(outgoing, "ep", split_axis=0, concat_axis=0, tiled=True)
    piece = lax.all_gather(arrived, "tp", axis=1, tiled=True)
    cols = piece.shape[1]
    part = piece.reshape(n_expdev, exp_dev, capacity, cols)
    gate_pre = jnp.einsum("sjcd,jdf->sjcf", part, w_gate_exp, preferred_element_type=jnp.float32)
    up_pre = jnp.einsum("sjcd,jdf->sjcf", part, w_up_exp, preferred_element_type=jnp.float32)
    hidden = (jax.nn.silu(gate_pre) * up_pre).astype(jnp.bfloat16)
    shared_hidden = (
        jax.nn.silu(jnp.dot(normed_second, w_gate_shared, preferred_element_type=jnp.float32))
        * jnp.dot(normed_second, w_up_shared, preferred_element_type=jnp.float32)
    ).astype(jnp.bfloat16)
    routed_term = jnp.einsum(
        "sjcf,jfd->dsjc", hidden, w_down_exp, preferred_element_type=jnp.float32
    ).reshape(lax.axis_size("tp") * (MODEL_WIDTH // lax.axis_size("tp")), slot_count)
    shared_term = lax.dot_general(
        w_down_shared, shared_hidden, (((0,), (1,)), ((), ())), preferred_element_type=jnp.float32
    )
    summed = lax.psum_scatter(
        jnp.concatenate([routed_term, shared_term], axis=1).astype(jnp.bfloat16),
        "tp",
        scatter_dimension=0,
        tiled=True,
    ).astype(jnp.float32)
    routed_part = summed[:, :slot_count].astype(jnp.bfloat16)
    returned = lax.all_to_all(routed_part, "ep", split_axis=1, concat_axis=1, tiled=True)
    weighted = lax.dot_general(
        combine,
        returned.astype(jnp.float32),
        (((0,), (1,)), ((), ())),
        precision=lax.Precision.HIGHEST,
    )
    moe_out = (weighted + summed[:, slot_count:].T).astype(jnp.bfloat16)
    return (mixer_out, moe_out)


def solution(mesh):
    in_specs = (
        P("ep", None),
        P(),
        P(None, "tp"),
        P(None, "tp"),
        P(None, "tp"),
        P("tp"),
        P("tp", None),
        P("ep", None),
        P(),
        P("ep", None),
        P("ep", None),
        P("ep", None, "tp"),
        P("ep", None, "tp"),
        P("ep", "tp", None),
        P(None, "tp"),
        P(None, "tp"),
        P("tp", None),
    )
    out_specs = (P(("ep", "tp"), None), P("ep", "tp"))
    return jax.shard_map(local, mesh=mesh, in_specs=in_specs, out_specs=out_specs, check_vma=False)
```

profile of v0, /device:TPU:0, one launch (start us, length us, event | category | flops | bytes accessed | tf_op | source)
XLA Modules:
  0.0 194.5 jit_solution(10042323882435477261)
XLA Ops:
  7.2 0.0 copy-start
  7.2 0.0 all-gather.2.cloned.1.call-start
  7.2 0.9 copy.42
  8.2 0.1 eq.40
  8.3 0.1 eq.44
  8.4 1.2 reduce-window.6
  9.5 0.2 slice_reduce_fusion
  9.8 0.1 fusion.58
  9.9 0.1 reduce_sum.60
  10.0 0.1 copy.45
  10.1 0.7 multiply_add_fusion
  10.8 1.2 fusion.34
  12.0 1.2 convert_reduce_fusion
  13.2 1.2 fusion.36
  14.4 0.4 convolution_convert_fusion.2
  14.9 32.9 %all_to_all.24 = bf16[8,128,512]{2,1,0:T(8,128)(2,1)} all-to-all(bf16[8,128,512]{2,1,0:T(8,128)(2,1)S(1)} %bitcast.121), channel_id=1, replica_groups=mesh['ep'=8,'tp'=4] {'ep'}, dimensions={0} | all-to-all | bytes 2097152 | tf_op jit(solution)/shard_map/all_to_all | solution.py:144
  47.8 0.0 all-gather.2.cloned.1.call-update
  47.8 0.0 reduce-scatter.5.cloned.1.call-start
  47.9 0.3 fusion.73
  48.2 2.3 %fusion.16 = bf16[2048,128]{0,1:T(8,128)(2,1)S(1)} fusion(bf16[256,2048]{1,0:T(8,128)(2,1)} %param.33, bf16[128,2048]{1,0:T(8,128)(2,1)S(1)} %fusion.36, bf16[2048,256]{1,0:T(8,128)(2,1)} %param.32, f32[128,256]{1,0:T(8,128)S(1)} %fusion.73), kind=kOutput, calls=%fused_computation.23 | convolution fusion | flops 268894208 | bytes 3276800 | tf_op jit(solution)/shard_map/dot_general | solution.py:158
  50.5 30.9 %all-gather.2.cloned.1.call-done = bf16[1024,2048]{1,0:T(8,128)(2,1)} async-done(((bf16[1024,512]{1,0:T(8,128)(2,1)}), bf16[1024,2048]{1,0:T(8,128)(2,1)}) %all-gather.2.cloned.1.call-update) | async-done | bytes 4194320 | tf_op jit(solution)/shard_map/all_gather | solution.py:145
  81.5 7.2 %fusion.8 = f32[2,8,64,512]{3,2,1,0:T(8,128)} fusion(bf16[2,2048,512]{2,1,0:T(8,128)(2,1)} %param.28, bf16[8,2,64,2048]{3,2,1,0:T(8,128)(2,1)} %bitcast.130), kind=kOutput, calls=%fused_computation.14 | convolution fusion | flops 2147483648 | bytes 10485760 | tf_op jit(solution)/shard_map/sjcd,jdf->sjcf/dot_general | solution.py:148
  88.7 11.8 %convert_bitcast_fusion = bf16[2048,8,2,64]{0,3,1,2:T(8,128)(2,1)} fusion(bf16[2,512,2048]{2,1,0:T(8,128)(2,1)} %param.30, f32[2,8,64,512]{3,2,1,0:T(8,128)} %fusion.8, bf16[2,2048,512]{2,1,0:T(8,128)(2,1)} %param.29, bf16[8,2,64,2048]{3,2,1,0:T(8,128)(2,1)} %bitcast.131), kind=kOutput, calls=%fused_computation.16 | convolution fusion | flops 4300210176 | bytes 18874368 | tf_op jit(solution)/shard_map/sjcf,jfd->dsjc/dot_general | solution.py:155
  100.5 2.5 %copy.48 = bf16[2048,8,2,64]{0,3,2,1:T(8,128)(2,1)S(1)} copy(bf16[2048,8,2,64]{0,3,1,2:T(8,128)(2,1)} %convert_bitcast_fusion) | data formatting | bytes 8388608 | tf_op jit(solution)/shard_map/sjcf,jfd->dsjc/transpose | solution.py:155
  103.0 2.5 %pad_maximum_fusion = bf16[2048,1152]{0,1:T(8,128)(2,1)} fusion(bf16[2048,128]{0,1:T(8,128)(2,1)S(1)} %fusion.16, bf16[2048,1024]{0,1:T(8,128)(2,1)S(1)} %bitcast.118), kind=kLoop, calls=%fused_computation.5 | loop fusion | flops 9437184 | bytes 9437184 | tf_op jit(solution)/shard_map/concatenate | solution.py:162
  105.5 0.0 reduce-scatter.5.cloned.1.call-update
  105.5 0.0 reduce-scatter.3.cloned.1.call-start
  105.6 2.2 %fusion.1 = f32[512]{0:T(512)S(1)} fusion(bf16[512,2048]{1,0:T(8,128)(2,1)} %param.17), kind=kLoop, calls=%fused_computation.7 | loop fusion | flops 3145216 | bytes 2099200 | tf_op jit(solution)/shard_map/reduce_sum | solution.py:21
  107.9 0.3 multiply_cosine_fusion
  108.2 2.6 %fusion.70 = f32[512,128]{0,1:T(8,128)S(1)} fusion(bf16[2048,128]{1,0:T(8,128)(2,1)S(1)} %copy-done.4, bf16[512,2048]{1,0:T(8,128)(2,1)} %param.17, f32[2048]{0:T(1024)S(1)} %copy-done.5, f32[512]{0:T(512)S(1)} %add_rsqrt_fusion), kind=kOutput, calls=%fused_computation.105 | convolution fusion | flops 272629760 | bytes 2893824 | tf_op jit(solution)/shard_map/dot_general | solution.py:70
  110.9 4.0 %collective-permute-start.1 = (bf16[128,2,64]{0,2,1:T(8,128)(2,1)S(1)}, bf16[128,2,64]{0,2,1:T(8,128)(2,1)}, u32[]{:S(2)}, u32[]{:S(2)}) collective-permute-start(bf16[128,2,64]{0,2,1:T(8,128)(2,1)S(1)} %pad_maximum_fusion.1), channel_id=1, source_target_pairs={{0,4},{4,8},{8,12},{12,16},{16,20},{20,24},{24,28},{1,5},{5,9},{9,... | collective-permute-start | bytes 98312 | tf_op jit(solution)/shard_map/ppermute | solution.py:16
  114.8 2.1 %convolution_convert_fusion.3 = bf16[512,128]{0,1:T(8,128)(2,1)S(1)} fusion(bf16[2048,128]{1,0:T(8,128)(2,1)} %param.21, bf16[512,2048]{1,0:T(8,128)(2,1)S(1)} %copy-done.1, f32[2048]{0:T(1024)S(1)} %copy-done.5, f32[512]{0:T(512)S(1)} %add_rsqrt_fusion), kind=kOutput, calls=%fused_computation.43 | convolution fusion | flops 272695296 | bytes 2762752 | tf_op jit(solution)/shard_map/dot_general | solution.py:76
  116.9 3.6 %collective-permute-start = (bf16[128,2,64]{0,2,1:T(8,128)(2,1)S(1)}, bf16[128,2,64]{0,2,1:T(8,128)(2,1)}, u32[]{:S(2)}, u32[]{:S(2)}) collective-permute-start(bf16[128,2,64]{0,2,1:T(8,128)(2,1)S(1)} %bitcast.128), channel_id=1, source_target_pairs={{0,4},{4,8},{8,12},{12,16},{16,20},{20,24},{24,28},{1,5},{5,9},{9,... | collective-permute-start | bytes 98312 | tf_op jit(solution)/shard_map/ppermute | solution.py:16
  120.5 2.5 %fusion.68 = f32[512,256]{0,1:T(8,128)S(1)} fusion(bf16[2048,256]{1,0:T(8,128)(2,1)S(1)} %copy-done.3, bf16[512,2048]{1,0:T(8,128)(2,1)} %param.17, f32[2048]{0:T(1024)S(1)} %copy-done.5, f32[512]{0:T(512)S(1)} %add_rsqrt_fusion), kind=kOutput, calls=%fused_computation.104 | convolution fusion | flops 541065216 | bytes 3680256 | tf_op jit(solution)/shard_map/dot_general | solution.py:64
  123.0 0.1 subtract_convert_fusion
  123.1 0.4 fusion.30
  123.6 0.1 max.22
  123.6 1.8 fusion.10
  125.5 0.1 broadcast_maximum_fusion
  125.6 1.1 fusion
  126.7 0.1 exponential_add_fusion
  126.8 2.4 %fusion.31 = bf16[2,64,2,512]{3,1,2,0:T(8,128)(2,1)S(1)} fusion(f32[2,640,512,2]{2,1,3,0:T(8,128)S(1)} %get-tuple-element.32, f32[2,2,512]{2,1,0:T(2,128)S(1)} %exponential_add_fusion, f32[2,2,512]{2,1,0:T(2,128)S(1)} %broadcast_maximum_fusion, pred[512,640]{0,1:T(8,128)(4,1)S(1)} %fusion.30, bf16[512,2,64]{0,2,1:T(8,128)(2,1)S(1)} %bitcast.129, ...), kind=kOutput, calls=%fused_computation.41 | convolution fusion | flops 174784512 | bytes 6012928 | tf_op jit(solution)/shard_map/while/body/eval_jaxpr/hgqk,khd->qhgd/dot_general | solution.py:108
  129.2 2.1 %convolution_convert_fusion = bf16[512,2048]{1,0:T(8,128)(2,1)} fusion(bf16[512,256]{0,1:T(8,128)(2,1)S(1)} %bitcast.123, bf16[256,2048]{1,0:T(8,128)(2,1)S(1)} %copy-done), kind=kOutput, calls=%fused_computation.20 | convolution fusion | flops 537919488 | bytes 3407872 | tf_op jit(solution)/shard_map/dot_general | solution.py:117
  131.3 0.0 reduce-scatter.3.cloned.1.call-update
  131.4 22.1 %reduce-scatter.5.cloned.1.call-done = bf16[512,1152]{0,1:T(8,128)(2,1)} async-done(((bf16[2048,1152]{0,1:T(8,128)(2,1)}), bf16[512,1152]{0,1:T(8,128)(2,1)}) %reduce-scatter.5.cloned.1.call-update) | async-done | bytes 1179664 | tf_op jit(solution)/shard_map/reduce_scatter | solution.py:161
  153.5 1.3 slice.32
  154.8 30.9 %all_to_all.25 = bf16[512,8,128]{0,2,1:T(8,128)(2,1)S(1)} all-to-all(bf16[512,8,128]{0,2,1:T(8,128)(2,1)S(1)} %bitcast.122), channel_id=1, replica_groups=mesh['ep'=8,'tp'=4] {'ep'}, dimensions={1} | all-to-all | bytes 2097152 | tf_op jit(solution)/shard_map/all_to_all | solution.py:168
  185.7 2.3 %fusion.32 = bf16[128,512]{1,0:T(8,128)(2,1)} fusion(f32[1024,128]{1,0:T(8,128)S(1)} %get-tuple-element.17, bf16[512,1024]{0,1:T(8,128)(2,1)S(1)} %bitcast.119, bf16[512,1152]{0,1:T(8,128)(2,1)} %reduce-scatter.5.cloned.1.call-done), kind=kOutput, calls=%fused_computation.44 | convolution fusion | flops 805502976 | bytes 1835008 | tf_op jit(solution)/shard_map/dot_general | solution.py:169
  (29 shorter events, 0.2 us)
Async XLA Ops:
  7.2 122.1 %copy-start = (bf16[256,2048]{1,0:T(8,128)(2,1)S(1)}, bf16[256,2048]{1,0:T(8,128)(2,1)}, u32[]{:S(2)}) copy-start(bf16[256,2048]{1,0:T(8,128)(2,1)} %param.23) | copy-start | bytes 3145732
  7.2 40.7 %copy-start.2 = (bf16[2048,256]{1,0:T(8,128)(2,1)S(1)}, bf16[2048,256]{1,0:T(8,128)(2,1)}, u32[]{:S(2)}) copy-start(bf16[2048,256]{1,0:T(8,128)(2,1)} %param.31) | copy-start | bytes 3145732
  7.2 74.3 %all-gather.2.cloned.1.call-start = ((), (), s32[]{:S(2)}) async-start(), calls=%async_computation.5 | async-start | bytes 5242880 | tf_op jit(solution)/shard_map/all_gather | solution.py:145
  47.8 105.6 %reduce-scatter.5.cloned.1.call-start = ((), (), s32[]{:S(2)}) async-start(), calls=%async_computation.6 | async-start | bytes 5898240 | tf_op jit(solution)/shard_map/reduce_scatter | solution.py:161
  105.5 2.7 %copy-start.4 = (bf16[2048,128]{1,0:T(8,128)(2,1)S(1)}, bf16[2048,128]{1,0:T(8,128)(2,1)}, u32[]{:S(2)}) copy-start(bf16[2048,128]{1,0:T(8,128)(2,1)} %param.20) | copy-start | bytes 1572868
  105.5 2.7 %copy-start.5 = (f32[2048]{0:T(1024)S(1)}, f32[2048]{0:T(1024)}, u32[]{:S(2)}) copy-start(f32[2048]{0:T(1024)} %param.18) | copy-start | bytes 24580
  105.5 82.5 %reduce-scatter.3.cloned.1.call-start = ((), (), s32[]{:S(2)}) async-start(), calls=%async_computation.4 | async-start | bytes 2621440 | tf_op jit(solution)/shard_map/reduce_scatter | solution.py:116
  105.6 9.3 %copy-start.1 = (bf16[512,2048]{1,0:T(8,128)(2,1)S(1)}, bf16[512,2048]{1,0:T(8,128)(2,1)}, u32[]{:S(2)}) copy-start(bf16[512,2048]{1,0:T(8,128)(2,1)} %param.17) | copy-start | bytes 6291460
  108.2 12.3 %copy-start.3 = (bf16[2048,256]{1,0:T(8,128)(2,1)S(1)}, bf16[2048,256]{1,0:T(8,128)(2,1)}, u32[]{:S(2)}) copy-start(bf16[2048,256]{1,0:T(8,128)(2,1)} %param.19) | copy-start | bytes 3145732
  110.9 12.8 %collective-permute-start.1 = (bf16[128,2,64]{0,2,1:T(8,128)(2,1)S(1)}, bf16[128,2,64]{0,2,1:T(8,128)(2,1)}, u32[]{:S(2)}, u32[]{:S(2)}) collective-permute-start(bf16[128,2,64]{0,2,1:T(8,128)(2,1)S(1)} %pad_maximum_fusion.1), channel_id=1, source_target_pairs={{0,4},{4,8},{8,12},{12,16},{16,20},{20,24},{24,28},{1,5},{5,9},{9,... | collective-permute-start | bytes 98312 | tf_op jit(solution)/shard_map/ppermute | solution.py:16
  116.9 6.7 %copy-start.6 = (f32[4]{0:T(128)S(1)}, f32[4]{0:T(128)}, u32[]{:S(2)}) copy-start(f32[4]{0:T(128)} %param.22) | copy-start | bytes 52
  116.9 9.9 %collective-permute-start = (bf16[128,2,64]{0,2,1:T(8,128)(2,1)S(1)}, bf16[128,2,64]{0,2,1:T(8,128)(2,1)}, u32[]{:S(2)}, u32[]{:S(2)}) collective-permute-start(bf16[128,2,64]{0,2,1:T(8,128)(2,1)S(1)} %bitcast.128), channel_id=1, source_target_pairs={{0,4},{4,8},{8,12},{12,16},{16,20},{20,24},{24,28},{1,5},{5,9},{9,... | collective-permute-start | bytes 98312 | tf_op jit(solution)/shard_map/ppermute | solution.py:16
Sparse Core Ops, SparseCore 0:
  48.0 33.4 all-gather.1
  105.6 47.7 reduce-scatter.4
  156.6 31.1 reduce-scatter.2
where the time goes:
time: 195 us
  blocking collectives  63.9 us (33%)
  waiting for transfers between devices  53.1 us (27%)
  matrix products  37.9 us (19%)
  between operations  14 us (7%)
  other arithmetic  12.5 us (6%)
  starting transfers between devices  7.63 us (4%)
  local copies, waits for them, and re-layouts  5.45 us (3%)
    all_to_all x1, blocking collectives, local(): lax.all_to_all(outgoing, 'ep', split_axis=0, concat_axis=0, tiled=True)  32.9 us
    all_gather x1, waiting for transfers between devices, local(): piece = lax.all_gather(arrived, 'tp', axis=1, tiled=True)  30.9 us
    all_to_all x1, blocking collectives, local(): lax.all_to_all(routed_part, 'ep', split_axis=1, concat_axis=1, tiled=True)  30.9 us
    reduce_scatter x1, waiting for transfers between devices, local(): lax.psum_scatter(jnp.concatenate([routed_term, shared_term], axis=1).asty...  22.1 us
    dot_general x1, matrix products, local(): jnp.einsum('sjcf,jfd->dsjc', hidden, w_down_exp, preferred_element_type=j...  11.8 us
    ppermute x2, starting transfers between devices, from_behind(): return lax.ppermute(value, axis, pairs)  7.51 us
    dot_general x1, matrix products, local(): jnp.einsum('sjcd,jdf->sjcf', part, w_gate_exp, preferred_element_type=jnp...  7.19 us
  transfers between devices with their start and end apart: 5, of which 2 were waited for; matrix products, arithmetic and copies ran while one was open for 12% of the time, Pallas kernels for 0%

commit v1 on v0

--- a/solution.py
+++ b/solution.py
@@ -142,7 +142,9 @@
         jnp.bfloat16
     )
     arrived = lax.all_to_all(outgoing, "ep", split_axis=0, concat_axis=0, tiled=True)
-    piece = lax.all_gather(arrived, "tp", axis=1, tiled=True)
+    piece = jnp.concatenate(
+        lax.all_to_all(jnp.stack([arrived] * lax.axis_size("tp")), "tp", 0, 0), axis=1
+    )
     cols = piece.shape[1]
     part = piece.reshape(n_expdev, exp_dev, capacity, cols)
     gate_pre = jnp.einsum("sjcd,jdf->sjcf", part, w_gate_exp, preferred_element_type=jnp.float32)

time: 195 us -> 230 us (1.18)
  local copies, waits for them, and re-layouts: 5.45 us -> 22.8 us
  waiting for transfers between devices: 53.1 us -> 66.8 us
  starting transfers between devices: 7.63 us -> 11.1 us
    all_to_all x0 -> x1, waiting for transfers between devices: none -> 44.1 us  [local(): lax.all_to_all(jnp.stack([arrived] * lax.axis_size('tp')), 'tp', 0, 0)]
    all_gather x1 -> x0, waiting for transfers between devices: 30.9 us -> none  [local(): piece = lax.all_gather(arrived, 'tp', axis=1, tiled=True)]
    another operation x1 -> x3, local copies, waits for them, and re-layouts: 0.01 us -> 10 us  [the longest x1 7.75 us: local(): part = piece.reshape(n_expdev, exp_dev, capacity, cols)]
    reshape x0 -> x1, local copies, waits for them, and re-layouts: none -> 7.39 us  [local(): jnp.concatenate(lax.all_to_all(jnp.stack([arrived] * lax.axis_size('tp'))...]
    all_to_all x0 -> x1, starting transfers between devices: none -> 4.86 us  [local(): lax.all_to_all(jnp.stack([arrived] * lax.axis_size('tp')), 'tp', 0, 0)]
  transfers between devices with their start and end apart: 5 -> 5, of which waited for: 2 -> 2; matrix products, arithmetic and copies ran while one was open for 12% -> 11% of each run, Pallas kernels for 0% -> 0%
where the time goes in v1:
time: 230 us
  waiting for transfers between devices  66.8 us (29%)
  blocking collectives  63.7 us (28%)
  matrix products  38.3 us (17%)
  local copies, waits for them, and re-layouts  22.8 us (10%)
  between operations  14.3 us (6%)
  other arithmetic  12.5 us (5%)
  starting transfers between devices  11.1 us (5%)
    all_to_all x1, waiting for transfers between devices, local(): lax.all_to_all(jnp.stack([arrived] * lax.axis_size('tp')), 'tp', 0, 0)  44.1 us
    all_to_all x1, blocking collectives, local(): lax.all_to_all(outgoing, 'ep', split_axis=0, concat_axis=0, tiled=True)  32.8 us
    all_to_all x1, blocking collectives, local(): lax.all_to_all(routed_part, 'ep', split_axis=1, concat_axis=1, tiled=True)  30.9 us
    reduce_scatter x1, waiting for transfers between devices, local(): lax.psum_scatter(jnp.concatenate([routed_term, shared_term], axis=1).asty...  22.6 us
    dot_general x1, matrix products, local(): jnp.einsum('sjcf,jfd->dsjc', hidden, w_down_exp, preferred_element_type=j...  11.8 us
    another operation x1, local copies, waits for them, and re-layouts, local(): part = piece.reshape(n_expdev, exp_dev, capacity, cols)  7.75 us
    reshape x1, local copies, waits for them, and re-layouts, local(): jnp.concatenate(lax.all_to_all(jnp.stack([arrived] * lax.axis_size('tp'))...  7.39 us
    dot_general x1, matrix products, local(): jnp.einsum('sjcd,jdf->sjcf', part, w_gate_exp, preferred_element_type=jnp...  7.19 us
  transfers between devices with their start and end apart: 5, of which 2 were waited for; matrix products, arithmetic and copies ran while one was open for 11% of the time, Pallas kernels for 0%

profile of v1, /device:TPU:0, one launch (start us, length us, event | category | flops | bytes accessed | tf_op | source)
XLA Modules:
  0.0 229.6 jit_solution(14351808855409867024)
XLA Ops:
  7.2 0.9 copy.54
  8.1 0.1 eq.40
  8.2 0.1 eq.44
  8.3 1.2 reduce-window.6
  9.4 0.2 slice_reduce_fusion
  9.7 0.1 fusion.58
  9.8 0.1 reduce_sum.60
  9.9 0.1 copy.57
  10.0 0.7 multiply_add_fusion
  10.7 1.2 fusion.34
  11.9 1.2 convert_reduce_fusion
  13.1 1.2 fusion.36
  14.3 0.4 convolution_convert_fusion.2
  14.8 32.8 %all_to_all.26 = bf16[8,128,512]{2,1,0:T(8,128)(2,1)S(1)} all-to-all(bf16[8,128,512]{2,1,0:T(8,128)(2,1)S(1)} %bitcast.121), channel_id=1, replica_groups=mesh['ep'=8,'tp'=4] {'ep'}, dimensions={0} | all-to-all | bytes 2097152 | tf_op jit(solution)/shard_map/all_to_all | solution.py:144
  47.6 2.3 stack.10
  49.9 4.9 %all-to-all-start.1 = ((bf16[4,1024,512]{2,1,0:T(8,128)(2,1)}), bf16[4,1024,512]{2,1,0:T(8,128)(2,1)}, u32[]{:S(2)}, u32[]{:S(2)}) async-start(bf16[4,1024,512]{2,1,0:T(8,128)(2,1)} %stack.10), calls=%async_computation.2 | async-start | bytes 8388608 | tf_op jit(solution)/shard_map/all_to_all | solution.py:146
  54.8 0.2 reduce-scatter.5.cloned.1.call-start
  55.0 1.5 fusion.73
  56.5 2.3 %fusion.16 = bf16[2048,128]{0,1:T(8,128)(2,1)S(1)} fusion(bf16[256,2048]{1,0:T(8,128)(2,1)} %param.33, bf16[128,2048]{1,0:T(8,128)(2,1)S(1)} %fusion.36, bf16[2048,256]{1,0:T(8,128)(2,1)} %param.32, f32[128,256]{1,0:T(8,128)S(1)} %fusion.73), kind=kOutput, calls=%fused_computation.23 | convolution fusion | flops 268894208 | bytes 3276800 | tf_op jit(solution)/shard_map/dot_general | solution.py:160
  58.9 44.1 %all-to-all-done.1 = bf16[4,1024,512]{2,1,0:T(8,128)(2,1)} async-done(((bf16[4,1024,512]{2,1,0:T(8,128)(2,1)}), bf16[4,1024,512]{2,1,0:T(8,128)(2,1)}, u32[]{:S(2)}, u32[]{:S(2)}) %all-to-all-start.1) | async-done | bytes 4194336 | tf_op jit(solution)/shard_map/all_to_all | solution.py:146
  103.0 7.4 %copy.58 = bf16[1024,4,512]{2,1,0:T(4,128)(2,1)} copy(bf16[1024,4,512]{2,0,1:T(8,128)(2,1)} %bitcast.16) | data formatting | bytes 8388608 | tf_op jit(solution)/shard_map/reshape | solution.py:145
  110.4 7.7 %reshape_reshape.3 = bf16[8,2,64,2048]{3,2,1,0:T(8,128)(2,1)} reshape(bf16[1024,4,512]{2,1,0:T(4,128)(2,1)} %copy.58) | data formatting | bytes 8388608 | tf_op jit(solution)/shard_map/reshape;reshape | solution.py:149
  118.1 7.2 %fusion.8 = f32[2,8,64,512]{3,2,1,0:T(8,128)} fusion(bf16[2,2048,512]{2,1,0:T(8,128)(2,1)} %param.28, bf16[8,2,64,2048]{3,2,1,0:T(8,128)(2,1)} %reshape_reshape.3), kind=kOutput, calls=%fused_computation.14 | convolution fusion | flops 2147483648 | bytes 10485760 | tf_op jit(solution)/shard_map/sjcd,jdf->sjcf/dot_general | solution.py:150
  125.3 11.8 %convert_bitcast_fusion = bf16[2048,8,2,64]{0,3,1,2:T(8,128)(2,1)} fusion(bf16[2,512,2048]{2,1,0:T(8,128)(2,1)} %param.30, f32[2,8,64,512]{3,2,1,0:T(8,128)} %fusion.8, bf16[2,2048,512]{2,1,0:T(8,128)(2,1)} %param.29, bf16[8,2,64,2048]{3,2,1,0:T(8,128)(2,1)} %reshape_reshape.3), kind=kOutput, calls=%fused_computation.16 | convolution fusion | flops 4300210176 | bytes 18874368 | tf_op jit(solution)/shard_map/sjcf,jfd->dsjc/dot_general | solution.py:157
  137.1 2.5 %copy.61 = bf16[2048,8,2,64]{0,3,2,1:T(8,128)(2,1)S(1)} copy(bf16[2048,8,2,64]{0,3,1,2:T(8,128)(2,1)} %convert_bitcast_fusion) | data formatting | bytes 8388608 | tf_op jit(solution)/shard_map/sjcf,jfd->dsjc/transpose | solution.py:157
  139.6 2.5 %pad_maximum_fusion = bf16[2048,1152]{0,1:T(8,128)(2,1)} fusion(bf16[2048,128]{0,1:T(8,128)(2,1)S(1)} %fusion.16, bf16[2048,1024]{0,1:T(8,128)(2,1)S(1)} %bitcast.118), kind=kLoop, calls=%fused_computation.5 | loop fusion | flops 9437184 | bytes 9437184 | tf_op jit(solution)/shard_map/concatenate | solution.py:164
  142.1 0.0 reduce-scatter.5.cloned.1.call-update
  142.1 0.0 reduce-scatter.3.cloned.1.call-start
  142.2 2.2 fusion.1
  144.5 0.3 multiply_cosine_fusion
  144.8 3.1 %fusion.70 = f32[512,128]{0,1:T(8,128)S(1)} fusion(bf16[2048,128]{1,0:T(8,128)(2,1)S(1)} %copy-done.2, bf16[512,2048]{1,0:T(8,128)(2,1)} %param.17, f32[2048]{0:T(1024)S(1)} %copy-done.3, f32[512]{0:T(512)S(1)} %add_rsqrt_fusion), kind=kOutput, calls=%fused_computation.105 | convolution fusion | flops 272629760 | bytes 2893824 | tf_op jit(solution)/shard_map/dot_general | solution.py:70
  148.0 3.2 %collective-permute-start.1 = (bf16[128,2,64]{0,2,1:T(8,128)(2,1)S(1)}, bf16[128,2,64]{0,2,1:T(8,128)(2,1)S(1)}, u32[]{:S(2)}, u32[]{:S(2)}) collective-permute-start(bf16[128,2,64]{0,2,1:T(8,128)(2,1)S(1)} %pad_maximum_fusion.1), channel_id=1, source_target_pairs={{0,4},{4,8},{8,12},{12,16},{16,20},{20,24},{24,28},{1,5},{5,9},{9,... | collective-permute-start | bytes 98312 | tf_op jit(solution)/shard_map/ppermute | solution.py:16
  151.2 2.0 convolution_convert_fusion.3
  153.2 2.8 %collective-permute-start = (bf16[128,2,64]{0,2,1:T(8,128)(2,1)S(1)}, bf16[128,2,64]{0,2,1:T(8,128)(2,1)S(1)}, u32[]{:S(2)}, u32[]{:S(2)}) collective-permute-start(bf16[128,2,64]{0,2,1:T(8,128)(2,1)S(1)} %bitcast.128), channel_id=1, source_target_pairs={{0,4},{4,8},{8,12},{12,16},{16,20},{20,24},{24,28},{1,5},{5,9},{9,... | collective-permute-start | bytes 98312 | tf_op jit(solution)/shard_map/ppermute | solution.py:16
  156.0 2.8 %fusion.68 = f32[512,256]{0,1:T(8,128)S(1)} fusion(bf16[2048,256]{1,0:T(8,128)(2,1)} %param.19, bf16[512,2048]{1,0:T(8,128)(2,1)} %param.17, f32[2048]{0:T(1024)S(1)} %copy-done.3, f32[512]{0:T(512)S(1)} %add_rsqrt_fusion), kind=kOutput, calls=%fused_computation.104 | convolution fusion | flops 541065216 | bytes 3680256 | tf_op jit(solution)/shard_map/dot_general | solution.py:64
  158.8 0.1 subtract_convert_fusion
  158.9 0.4 fusion.30
  159.3 0.1 max.22
  159.4 1.1 fusion.10
  160.5 0.1 broadcast_maximum_fusion
  160.6 1.1 fusion
  161.7 0.1 exponential_add_fusion
  161.8 1.6 fusion.31
  163.5 2.1 convolution_convert_fusion
  165.6 22.6 %reduce-scatter.5.cloned.1.call-done = bf16[512,1152]{0,1:T(8,128)(2,1)} async-done(((bf16[2048,1152]{0,1:T(8,128)(2,1)}), bf16[512,1152]{0,1:T(8,128)(2,1)}) %reduce-scatter.5.cloned.1.call-update) | async-done | bytes 1179664 | tf_op jit(solution)/shard_map/reduce_scatter | solution.py:163
  188.2 1.3 slice.32
  189.5 30.9 %all_to_all.27 = bf16[512,8,128]{0,2,1:T(8,128)(2,1)S(1)} all-to-all(bf16[512,8,128]{0,2,1:T(8,128)(2,1)S(1)} %bitcast.122), channel_id=1, replica_groups=mesh['ep'=8,'tp'=4] {'ep'}, dimensions={1} | all-to-all | bytes 2097152 | tf_op jit(solution)/shard_map/all_to_all | solution.py:170
  220.4 2.3 %fusion.32 = bf16[128,512]{1,0:T(8,128)(2,1)} fusion(f32[1024,128]{1,0:T(8,128)S(1)} %get-tuple-element.17, bf16[512,1024]{0,1:T(8,128)(2,1)S(1)} %bitcast.120, bf16[512,1152]{0,1:T(8,128)(2,1)} %reduce-scatter.5.cloned.1.call-done), kind=kOutput, calls=%fused_computation.44 | convolution fusion | flops 805502976 | bytes 1835008 | tf_op jit(solution)/shard_map/dot_general | solution.py:171
  (27 shorter events, 0.2 us)
Async XLA Ops:
  7.2 156.3 %copy-start = (bf16[256,2048]{1,0:T(8,128)(2,1)S(1)}, bf16[256,2048]{1,0:T(8,128)(2,1)}, u32[]{:S(2)}) copy-start(bf16[256,2048]{1,0:T(8,128)(2,1)} %param.23) | copy-start | bytes 3145732
  49.9 53.1 %all-to-all-start.1 = ((bf16[4,1024,512]{2,1,0:T(8,128)(2,1)}), bf16[4,1024,512]{2,1,0:T(8,128)(2,1)}, u32[]{:S(2)}, u32[]{:S(2)}) async-start(bf16[4,1024,512]{2,1,0:T(8,128)(2,1)} %stack.10), calls=%async_computation.2 | async-start | bytes 8388608 | tf_op jit(solution)/shard_map/all_to_all | solution.py:146
  54.8 133.5 %reduce-scatter.5.cloned.1.call-start = ((), (), s32[]{:S(2)}) async-start(), calls=%async_computation.6 | async-start | bytes 5898240 | tf_op jit(solution)/shard_map/reduce_scatter | solution.py:163
  142.1 2.7 %copy-start.2 = (bf16[2048,128]{1,0:T(8,128)(2,1)S(1)}, bf16[2048,128]{1,0:T(8,128)(2,1)}, u32[]{:S(2)}) copy-start(bf16[2048,128]{1,0:T(8,128)(2,1)} %param.20) | copy-start | bytes 1572868
  142.1 2.7 %copy-start.3 = (f32[2048]{0:T(1024)S(1)}, f32[2048]{0:T(1024)}, u32[]{:S(2)}) copy-start(f32[2048]{0:T(1024)} %param.18) | copy-start | bytes 24580
  142.1 80.6 %reduce-scatter.3.cloned.1.call-start = ((), (), s32[]{:S(2)}) async-start(), calls=%async_computation.5 | async-start | bytes 2621440 | tf_op jit(solution)/shard_map/reduce_scatter | solution.py:116
  142.2 9.0 %copy-start.1 = (bf16[512,2048]{1,0:T(8,128)(2,1)S(1)}, bf16[512,2048]{1,0:T(8,128)(2,1)}, u32[]{:S(2)}) copy-start(bf16[512,2048]{1,0:T(8,128)(2,1)} %param.17) | copy-start | bytes 6291460
  148.0 11.5 %collective-permute-start.1 = (bf16[128,2,64]{0,2,1:T(8,128)(2,1)S(1)}, bf16[128,2,64]{0,2,1:T(8,128)(2,1)S(1)}, u32[]{:S(2)}, u32[]{:S(2)}) collective-permute-start(bf16[128,2,64]{0,2,1:T(8,128)(2,1)S(1)} %pad_maximum_fusion.1), channel_id=1, source_target_pairs={{0,4},{4,8},{8,12},{12,16},{16,20},{20,24},{24,28},{1,5},{5,9},{9,... | collective-permute-start | bytes 98312 | tf_op jit(solution)/shard_map/ppermute | solution.py:16
  153.2 6.2 %copy-start.4 = (f32[4]{0:T(128)S(1)}, f32[4]{0:T(128)}, u32[]{:S(2)}) copy-start(f32[4]{0:T(128)} %param.22) | copy-start | bytes 52
  153.2 8.6 %collective-permute-start = (bf16[128,2,64]{0,2,1:T(8,128)(2,1)S(1)}, bf16[128,2,64]{0,2,1:T(8,128)(2,1)S(1)}, u32[]{:S(2)}, u32[]{:S(2)}) collective-permute-start(bf16[128,2,64]{0,2,1:T(8,128)(2,1)S(1)} %bitcast.128), channel_id=1, source_target_pairs={{0,4},{4,8},{8,12},{12,16},{16,20},{20,24},{24,28},{1,5},{5,9},{9,... | collective-permute-start | bytes 98312 | tf_op jit(solution)/shard_map/ppermute | solution.py:16
Sparse Core Ops, SparseCore 0:
  142.3 45.9 reduce-scatter.4
  191.3 31.1 reduce-scatter.2
